TPU v7x, 256 devices: a whole 4x4x8 slice. The times are simulated.
256 devices in a mesh: sp: 32 (over z, y), tp: 8 (over x, core).
Axes of the slice: x: 4, y: 4, z: 8, core: 2. Of those that a mesh axis runs over, the one named last changes fastest.
Arguments:
- latent: bfloat16 [16384, 4096], P(('sp', 'tp')), may hold values from -3 to 3
- context: bfloat16 [1024, 4096], P('sp'), may hold values from -6 to 6
- cond: float32 [4096], replicated, may hold values from -6 to 6
- ctx_cond: float32 [4096], replicated, may hold values from -6 to 6
- w_shift: bfloat16 [4096, 4096], P('sp', 'tp'), may hold values from -0.1875 to 0.1875
- w_scale: bfloat16 [4096, 4096], P('sp', 'tp'), may hold values from -0.09375 to 0.15478516
- w_gate: bfloat16 [4096, 4096], P('sp', 'tp'), may hold values from -0.1875 to 0.1875
- w_query: bfloat16 [4096, 2048], P(None, 'tp'), may hold values from -0.09375 to 0.09375
- key_weight: bfloat16 [4096, 1024], P(None, 'tp'), may hold values from -0.09375 to 0.09375
- value_weight: bfloat16 [4096, 1024], P(None, 'tp'), may hold values from -0.09375 to 0.09375
- w_out: bfloat16 [2048, 4096], P('tp'), may hold values from -0.125 to 0.125
- sink: float32 [16], replicated, may hold values from 4 to 8
Outputs:
- mixed: bfloat16 [16384, 4096], P(('sp', 'tp'))
All inputs are finite; a program needn't handle non-finite values.
Results may differ from a plain program's by a relative error of at most 0.035.
Values may be sent and summed in bfloat16 or wider, within the bound.
A program may use at most 64 MiB of HBM per device.

v0:
```python
import jax
import jax.numpy as jnp
from jax import lax
from jax.sharding import PartitionSpec as P

HEAD_SIZE = 128
WINDOW_SIDE = 128
GRID_WIDTH = 64
EPS = 1e-05
THETA = 10000.0
MASKED = -1e30


def sent_to_all(value, axis):
    length = lax.axis_size(axis)
    return lax.all_to_all(
        jnp.broadcast_to(value[None], (length, *value.shape)), axis, 0, 0, tiled=True
    )


def taken_together(value, axis):
    everything = sent_to_all(value, axis)
    return jnp.sum(everything, axis=0)


def in_one(arrays, axis):
    line, at, done = (jnp.concatenate([a.reshape(-1) for a in arrays]), 0, [])
    subtotal = taken_together(line, axis)
    for a in arrays:
        done.append(subtotal[at : at + a.size].reshape(a.shape))
        at += a.size
    return tuple(done)


def side_by_side(arrays, axis, dim, along):
    widths = [a.shape[along] for a in arrays]
    both = jnp.concatenate(arrays, axis=along)
    filled = lax.all_gather(both, axis, axis=dim, tiled=True)
    return tuple(jnp.split(filled, [sum(widths[:k]) for k in range(1, len(widths))], axis=along))


def in_order(tiles, dim):
    tiles = jnp.moveaxis(tiles, 0, dim)
    lengths = tiles.shape
    return tiles.reshape(*lengths[:dim], lengths[dim] * lengths[dim + 1], *lengths[dim + 2 :])


def gather_directly(value, axis, dim):
    tiles = sent_to_all(value, axis)
    return in_order(tiles, dim)


def with_halo(cells, sides, width):
    for axis, dim in sides:
        count = lax.axis_size(axis)
        ends = count - 1
        head = lax.slice_in_dim(cells, 0, width, axis=dim)
        tail = lax.slice_in_dim(cells, cells.shape[dim] - width, cells.shape[dim], axis=dim)
        cells = jnp.concatenate(
            [
                lax.ppermute(tail, axis, [(i, (i + 1) % count) for i in range(ends)]),
                cells,
                lax.ppermute(head, axis, [((i + 1) % count, i) for i in range(ends)]),
            ],
            axis=dim,
        )
    return cells


def layer_norm(rows):
    values = rows.astype(jnp.float32)
    mean = jnp.mean(values, axis=-1, keepdims=True)
    var = jnp.mean(jnp.square(values - mean), axis=-1, keepdims=True)
    return (values - mean) * lax.rsqrt(var + EPS)


def rotate_half(values, token_position, width):
    half = width // 2
    inverse = THETA ** (-jnp.arange(half, dtype=jnp.float32) * 2.0 / width)
    angle = token_position.astype(jnp.float32)[:, None] * inverse[None, :]
    cosine = jnp.cos(angle)[:, None, :]
    sine = jnp.sin(angle)[:, None, :]
    first = values[..., :half]
    second = values[..., half:]
    return jnp.concatenate(
        [first * cosine - second * sine, second * cosine + first * sine], axis=-1
    )


def axial_rotation(heads, token_position, grid):
    width = heads.shape[-1] // 2
    values = heads.astype(jnp.float32)
    turned = jnp.concatenate(
        [
            rotate_half(values[..., :width], token_position // grid, width),
            rotate_half(values[..., width:], token_position % grid, width),
        ],
        axis=-1,
    )
    return turned.astype(jnp.bfloat16)


def sink_weights(scores, sink_column):
    top = jnp.maximum(jnp.max(scores, axis=-1, keepdims=True), sink_column)
    expo = jnp.exp(scores - top)
    return (expo / (jnp.sum(expo, axis=-1, keepdims=True) + jnp.exp(sink_column - top))).astype(
        jnp.bfloat16
    )


def shards(
    latent,
    context,
    cond,
    ctx_cond,
    w_shift,
    w_scale,
    w_gate,
    w_query,
    key_weight,
    value_weight,
    w_out,
    sink,
):
    sp_count = lax.axis_size("sp")
    sp_index = lax.axis_index("sp")
    tp_index = lax.axis_index("tp")
    block_rows = w_shift.shape[0]
    act = jax.nn.silu(jnp.stack([cond, ctx_cond])).astype(jnp.bfloat16)
    own_act = lax.dynamic_slice_in_dim(act, sp_index * block_rows, block_rows, 1)
    shift_part = jnp.dot(own_act, w_shift, preferred_element_type=jnp.float32)
    scale_part = jnp.dot(own_act, w_scale, preferred_element_type=jnp.float32)
    gate_part = jnp.dot(own_act[0:1], w_gate, preferred_element_type=jnp.float32)
    shift_sum, scale_sum, gate_sum = in_one((shift_part, scale_part, gate_part), "sp")
    shift, scale, gate = side_by_side((shift_sum, scale_sum, gate_sum), "tp", 1, 0)
    latent_mod = (layer_norm(latent) * (1.0 + scale[0]) + shift[0]).astype(jnp.bfloat16)
    ctx_mod = (layer_norm(context) * (1.0 + scale[1]) + shift[1]).astype(jnp.bfloat16)
    kv_cols = key_weight.shape[1]
    q_cols = w_query.shape[1]
    ctx_pair = gather_directly(
        jnp.concatenate(
            [
                jnp.dot(ctx_mod, key_weight, preferred_element_type=jnp.float32).astype(
                    jnp.bfloat16
                ),
                jnp.dot(ctx_mod, value_weight, preferred_element_type=jnp.float32).astype(
                    jnp.bfloat16
                ),
            ],
            axis=1,
        ),
        "sp",
        0,
    )
    piece = lax.all_gather(latent_mod, "tp", axis=0, tiled=True)
    projected_rows = jnp.concatenate(
        [
            jnp.dot(piece, w_query, preferred_element_type=jnp.float32).astype(jnp.bfloat16),
            jnp.dot(piece, key_weight, preferred_element_type=jnp.float32).astype(jnp.bfloat16),
            jnp.dot(piece, value_weight, preferred_element_type=jnp.float32).astype(jnp.bfloat16),
        ],
        axis=1,
    )
    tokens_here = projected_rows.shape[0]
    kv_heads = kv_cols // HEAD_SIZE
    q_heads = q_cols // HEAD_SIZE
    query_group = q_heads // kv_heads
    offset = sp_index * tokens_here
    token_position = offset + jnp.arange(tokens_here, dtype=jnp.int32)
    query = axial_rotation(
        projected_rows[:, :q_cols].reshape(tokens_here, q_heads, HEAD_SIZE),
        token_position,
        GRID_WIDTH,
    )
    key = axial_rotation(
        projected_rows[:, q_cols : q_cols + kv_cols].reshape(tokens_here, kv_heads, HEAD_SIZE),
        token_position,
        GRID_WIDTH,
    )
    value_rows = projected_rows[:, q_cols + kv_cols :]
    extended = with_halo(
        jnp.concatenate([key.reshape(tokens_here, kv_cols), value_rows], axis=1),
        (("sp", 0),),
        WINDOW_SIDE,
    )
    block_list = tokens_here // WINDOW_SIDE
    band = jnp.concatenate(
        [
            extended[shift_index * WINDOW_SIDE : shift_index * WINDOW_SIDE + tokens_here].reshape(
                block_list, WINDOW_SIDE, 2 * kv_cols
            )
            for shift_index in range(3)
        ],
        axis=1,
    )
    band_key = band[..., :kv_cols].reshape(block_list, 3 * WINDOW_SIDE, kv_heads, HEAD_SIZE)
    band_value = band[..., kv_cols:].reshape(block_list, 3 * WINDOW_SIDE, kv_heads, HEAD_SIZE)
    context_key_rows = ctx_pair[:, :kv_cols].reshape(-1, kv_heads, HEAD_SIZE)
    context_value_rows = ctx_pair[:, kv_cols:].reshape(-1, kv_heads, HEAD_SIZE)
    query_block_list = query.reshape(block_list, WINDOW_SIDE, kv_heads, query_group, HEAD_SIZE)
    factor = HEAD_SIZE ** (-0.5)
    band_scores = (
        jnp.einsum(
            "nqhgd,nkhd->nhgqk", query_block_list, band_key, preferred_element_type=jnp.float32
        )
        * factor
    )
    total = tokens_here * sp_count
    qpos = token_position.reshape(block_list, WINDOW_SIDE)[:, :, None]
    kpos = (
        offset
        - WINDOW_SIDE
        + (jnp.arange(block_list, dtype=jnp.int32) * WINDOW_SIDE)[:, None, None]
        + jnp.arange(3 * WINDOW_SIDE, dtype=jnp.int32)[None, None, :]
    )
    valid = (jnp.abs(kpos - qpos) <= WINDOW_SIDE) & (kpos >= 0) & (kpos < total)
    band_scores = jnp.where(valid[:, None, None], band_scores, MASKED)
    ctx_scores = (
        jnp.einsum(
            "nqhgd,khd->nhgqk",
            query_block_list,
            context_key_rows,
            preferred_element_type=jnp.float32,
        )
        * factor
    )
    own_sink = lax.dynamic_slice_in_dim(sink, tp_index * q_heads, q_heads).reshape(
        kv_heads, query_group
    )[:, :, None, None]
    weights = sink_weights(jnp.concatenate([band_scores, ctx_scores], axis=-1), own_sink)
    attended = jnp.einsum(
        "nhgqk,nkhd->nqhgd",
        weights[..., : 3 * WINDOW_SIDE],
        band_value,
        preferred_element_type=jnp.float32,
    ) + jnp.einsum(
        "nhgqk,khd->nqhgd",
        weights[..., 3 * WINDOW_SIDE :],
        context_value_rows,
        preferred_element_type=jnp.float32,
    )
    attended = attended.astype(jnp.bfloat16).reshape(tokens_here, q_cols)
    projected = lax.psum_scatter(
        jnp.dot(attended, w_out, preferred_element_type=jnp.float32).astype(jnp.bfloat16),
        "tp",
        scatter_dimension=0,
        tiled=True,
    ).astype(jnp.float32)
    return (latent.astype(jnp.float32) + gate[0][None, :] * projected).astype(jnp.bfloat16)


def solution(mesh):
    in_specs = (
        P(("sp", "tp"), None),
        P("sp", None),
        P(),
        P(),
        P("sp", "tp"),
        P("sp", "tp"),
        P("sp", "tp"),
        P(None, "tp"),
        P(None, "tp"),
        P(None, "tp"),
        P("tp", None),
        P(),
    )
    out_specs = P(("sp", "tp"), None)
    return jax.shard_map(shards, mesh=mesh, in_specs=in_specs, out_specs=out_specs, check_vma=False)
```

profile of v0, /device:TPU:8, one launch (start us, length us, event | category | flops | bytes accessed | tf_op | source)
XLA Modules:
  0.0 172.2 jit_solution(11445464485622171272)
XLA Ops:
  7.4 1.1 fusion.50
  11.5 11.7 %all-to-all-start = ((f32[32,1,2560]{2,1,0:T(1,128)}), f32[32,1,2560]{2,1,0:T(1,128)}, u32[]{:S(2)}, u32[]{:S(2)}) async-start(f32[32,1,2560]{2,1,0:T(1,128)} %broadcast_in_dim.12), calls=%async_computation | async-start | bytes 655360 | tf_op jit(solution)/shard_map/all_to_all | solution.py:16
  23.3 1.2 convert_reduce_fusion
  24.6 1.3 fusion.10
  25.9 10.0 %all-to-all-done = f32[32,1,2560]{2,1,0:T(1,128)} async-done(((f32[32,1,2560]{2,1,0:T(1,128)}), f32[32,1,2560]{2,1,0:T(1,128)}, u32[]{:S(2)}, u32[]{:S(2)}) %all-to-all-start) | async-done | bytes 327712 | tf_op jit(solution)/shard_map/all_to_all | solution.py:16
  36.0 1.2 reduce_sum.54
  37.2 13.1 %all_gather.6 = f32[5,4096]{1,0:T(8,128)S(1)} all-gather(f32[5,512]{1,0:T(8,128)S(1)} %pad_maximum_fusion.4), channel_id=1, replica_groups=mesh['sp'=32,'tp'=8] {'tp'}, dimensions={1}, use_global_device_ids=true | all-gather | bytes 92160 | tf_op jit(solution)/shard_map/all_gather | solution.py:38
  50.4 2.1 %fusion.13 = bf16[64,4096]{1,0:T(8,128)(2,1)} fusion(bf16[64,4096]{1,0:T(8,128)(2,1)} %param.12, f32[4096]{0:T(1024)S(1)} %bitcast.140, f32[4096]{0:T(1024)S(1)} %bitcast.141, f32[64]{0:T(128)S(1)} %add_rsqrt_fusion.1, f32[64]{0:T(128)S(1)} %broadcast_multiply_fusion.1), kind=kLoop, calls=%fused_computation.30 | loop fusion | flops 1572864 | bytes 1081856 | tf_op jit(solution)/shard_map/convert_element_type | solution.py:136
  53.8 1.9 %fusion.16 = pred[4,128,384]{1,2,0:T(8,128)(4,1)} fusion(s32[4,128]{1,0:T(4,128)S(1)} %add_add_fusion, s32[4,384]{1,0:T(4,128)S(1)} %iota_add_fusion, pred[4,384]{1,0:T(4,128)(4,1)S(1)} %get-tuple-element.33, pred[4,384]{1,0:T(4,128)(4,1)S(1)} %get-tuple-element.32), kind=kLoop, calls=%fused_computation.36 | loop fusion | flops 983040 | bytes 207872 | tf_op jit(solution)/shard_map/and | solution.py:216
  55.7 1.2 multiply_cosine_fusion.1
  56.9 1.5 convolution_convert_fusion.4
  59.7 5.9 %all-to-all-start.1 = ((bf16[32,32,256]{2,1,0:T(8,128)(2,1)}), bf16[32,32,256]{2,1,0:T(8,128)(2,1)}, u32[]{:S(2)}, u32[]{:S(2)}) async-start(bf16[32,32,256]{2,1,0:T(8,128)(2,1)} %broadcast_in_dim.15), calls=%async_computation.1 | async-start | bytes 1048576 | tf_op jit(solution)/shard_map/all_to_all | solution.py:16
  65.6 17.7 %all-gather.2.cloned.1.call-done = bf16[512,4096]{1,0:T(8,128)(2,1)} async-done(((bf16[64,4096]{1,0:T(8,128)(2,1)}), bf16[512,4096]{1,0:T(8,128)(2,1)}) %all-gather.2.cloned.1.call-update) | async-done | bytes 4194320 | tf_op jit(solution)/shard_map/all_gather | solution.py:155
  83.3 3.7 %fusion.9 = f32[512,1,128]{0,2,1:T(8,128)S(1)} fusion(bf16[512,4096]{1,0:T(8,128)(2,1)} %all-gather.2.cloned.1.call-done, bf16[4096,128]{1,0:T(8,128)(2,1)S(1)} %copy-done.4), kind=kOutput, calls=%fused_computation.22 | convolution fusion | flops 537001984 | bytes 5505024 | tf_op jit(solution)/shard_map/dot_general | solution.py:159
  88.2 3.7 %convolution_convert_fusion.2 = bf16[512,128]{1,0:T(8,128)(2,1)S(1)} fusion(bf16[512,4096]{1,0:T(8,128)(2,1)} %all-gather.2.cloned.1.call-done, bf16[4096,128]{1,0:T(8,128)(2,1)} %param.21), kind=kOutput, calls=%fused_computation.19 | convolution fusion | flops 536936448 | bytes 5373952 | tf_op jit(solution)/shard_map/dot_general | solution.py:160
  92.9 3.4 %collective-permute-start = (bf16[128,256]{1,0:T(8,128)(2,1)}, bf16[128,256]{1,0:T(8,128)(2,1)}, u32[]{:S(2)}, u32[]{:S(2)}) collective-permute-start(bf16[128,256]{1,0:T(8,128)(2,1)} %get-tuple-element.19), channel_id=1, source_target_pairs={{0,8},{8,16},{16,24},{24,32},{32,40},{40,48},{48,56},{56,64},{64,7... | collective-permute-start | bytes 196616 | tf_op jit(solution)/shard_map/ppermute | solution.py:61
  96.3 3.3 %collective-permute-start.1 = (bf16[128,256]{1,0:T(8,128)(2,1)}, bf16[128,256]{1,0:T(8,128)(2,1)}, u32[]{:S(2)}, u32[]{:S(2)}) collective-permute-start(bf16[128,256]{1,0:T(8,128)(2,1)} %get-tuple-element.20), channel_id=1, source_target_pairs={{8,0},{16,8},{24,16},{32,24},{40,32},{48,40},{56,48},{64,56},{72,6... | collective-permute-start | bytes 196616 | tf_op jit(solution)/shard_map/ppermute | solution.py:63
  99.7 4.2 %convolution_convert_fusion.1 = bf16[512,256]{0,1:T(8,128)(2,1)S(1)} fusion(bf16[512,4096]{1,0:T(8,128)(2,1)} %all-gather.2.cloned.1.call-done, bf16[4096,256]{1,0:T(8,128)(2,1)} %param.19), kind=kOutput, calls=%fused_computation.17 | convolution fusion | flops 1073872896 | bytes 6553600 | tf_op jit(solution)/shard_map/dot_general | solution.py:158
  107.5 4.3 %fusion.59 = (f32[4,2,128]{2,1,0:T(2,128)}, f32[4,1,2,128,1024]{3,4,2,0,1:T(8,128)}) fusion(bf16[4,128,2,128]{3,1,2,0:T(8,128)(2,1)} %pad_maximum_fusion.3, bf16[1024,256]{1,0:T(8,128)(2,1)} %bitcast.31), kind=kOutput, calls=%fused_computation.123 | convolution fusion | flops 270531584 | bytes 4722688 | tf_op jit(solution)/shard_map/nqhgd,khd->nhgqk/dot_general | solution.py:219
  113.8 1.5 fusion.58
  117.5 1.4 fusion.7
  119.2 3.2 %convolution_convert_fusion = bf16[512,4096]{1,0:T(8,128)(2,1)} fusion(bf16[256,4096]{1,0:T(8,128)(2,1)S(1)} %copy-done, bf16[64,8,2,128]{3,2,1,0:T(2,128)(2,1)S(1)} %bitcast.122), kind=kOutput, calls=%fused_computation | convolution fusion | flops 1075838976 | bytes 6553600 | tf_op jit(solution)/shard_map/dot_general | solution.py:244
  122.4 40.9 %reduce-scatter.2.cloned.1.call-done = bf16[64,4096]{1,0:T(8,128)(2,1)} async-done(((bf16[512,4096]{1,0:T(8,128)(2,1)}), bf16[64,4096]{1,0:T(8,128)(2,1)}) %reduce-scatter.2.cloned.1.call-update) | async-done | bytes 524304 | tf_op jit(solution)/shard_map/reduce_scatter | solution.py:243
  163.4 2.0 %fusion.14 = bf16[64,4096]{1,0:T(8,128)(2,1)} fusion(bf16[64,4096]{1,0:T(8,128)(2,1)S(1)} %copy-done.2, bf16[64,4096]{1,0:T(8,128)(2,1)} %reduce-scatter.2.cloned.1.call-done, f32[4096]{0:T(1024)S(1)} %bitcast.139), kind=kLoop, calls=%fused_computation.31 | loop fusion | flops 1310720 | bytes 1589248 | tf_op jit(solution)/shard_map/convert_element_type | solution.py:249
  (109 shorter events, 16.5 us)
Async XLA Ops:
  6.5 112.6 %copy-start = (bf16[256,4096]{1,0:T(8,128)(2,1)S(1)}, bf16[256,4096]{1,0:T(8,128)(2,1)}, u32[]{:S(2)}) copy-start(bf16[256,4096]{1,0:T(8,128)(2,1)} %param.22) | copy-start | bytes 6291460
  6.5 46.0 %copy-start.20 = (f32[16]{0:T(128)S(1)}, f32[16]{0:T(128)}, u32[]{:S(2)}) copy-start(f32[16]{0:T(128)} %param.23) | copy-start | bytes 196
  6.5 46.7 %copy-start.3 = (bf16[32,4096]{1,0:T(8,128)(2,1)S(1)}, bf16[32,4096]{1,0:T(8,128)(2,1)}, u32[]{:S(2)}) copy-start(bf16[32,4096]{1,0:T(8,128)(2,1)} %param.13) | copy-start | bytes 786436
  6.5 51.9 %copy-start.4 = (bf16[4096,128]{1,0:T(8,128)(2,1)S(1)}, bf16[4096,128]{1,0:T(8,128)(2,1)}, u32[]{:S(2)}) copy-start(bf16[4096,128]{1,0:T(8,128)(2,1)} %param.20) | copy-start | bytes 3145732
  11.5 24.4 %all-to-all-start = ((f32[32,1,2560]{2,1,0:T(1,128)}), f32[32,1,2560]{2,1,0:T(1,128)}, u32[]{:S(2)}, u32[]{:S(2)}) async-start(f32[32,1,2560]{2,1,0:T(1,128)} %broadcast_in_dim.12), calls=%async_computation | async-start | bytes 655360 | tf_op jit(solution)/shard_map/all_to_all | solution.py:16
  23.3 60.0 %all-gather.2.cloned.1.call-start = ((), (), s32[]{:S(2)}) async-start(), calls=%async_computation.3 | async-start | bytes 4718592 | tf_op jit(solution)/shard_map/all_gather | solution.py:155
  59.7 47.8 %all-to-all-start.1 = ((bf16[32,32,256]{2,1,0:T(8,128)(2,1)}), bf16[32,32,256]{2,1,0:T(8,128)(2,1)}, u32[]{:S(2)}, u32[]{:S(2)}) async-start(bf16[32,32,256]{2,1,0:T(8,128)(2,1)} %broadcast_in_dim.15), calls=%async_computation.1 | async-start | bytes 1048576 | tf_op jit(solution)/shard_map/all_to_all | solution.py:16
  65.6 97.8 %reduce-scatter.2.cloned.1.call-start = ((), (), s32[]{:S(2)}) async-start(), calls=%async_computation.4 | async-start | bytes 4718592 | tf_op jit(solution)/shard_map/reduce_scatter | solution.py:243
  87.6 0.6 copy-start.10
  92.9 19.7 %collective-permute-start = (bf16[128,256]{1,0:T(8,128)(2,1)}, bf16[128,256]{1,0:T(8,128)(2,1)}, u32[]{:S(2)}, u32[]{:S(2)}) collective-permute-start(bf16[128,256]{1,0:T(8,128)(2,1)} %get-tuple-element.19), channel_id=1, source_target_pairs={{0,8},{8,16},{16,24},{24,32},{32,40},{40,48},{48,56},{56,64},{64,7... | collective-permute-start | bytes 196616 | tf_op jit(solution)/shard_map/ppermute | solution.py:61
  96.3 7.6 %copy-start.14 = (f32[512,32]{0,1:T(8,128)S(1)}, f32[512,32]{0,1:T(8,128)}, u32[]{:S(2)}) copy-start(f32[512,32]{0,1:T(8,128)} %get-tuple-element.28) | copy-start | bytes 196612
  96.3 7.6 %copy-start.15 = (f32[512,32]{0,1:T(8,128)S(1)}, f32[512,32]{0,1:T(8,128)}, u32[]{:S(2)}) copy-start(f32[512,32]{0,1:T(8,128)} %get-tuple-element.29) | copy-start | bytes 196612
  96.3 7.6 %copy-start.16 = (f32[512,32]{0,1:T(8,128)S(1)}, f32[512,32]{0,1:T(8,128)}, u32[]{:S(2)}) copy-start(f32[512,32]{0,1:T(8,128)} %get-tuple-element.34) | copy-start | bytes 196612
  96.3 7.6 %copy-start.17 = (f32[512,32]{0,1:T(8,128)S(1)}, f32[512,32]{0,1:T(8,128)}, u32[]{:S(2)}) copy-start(f32[512,32]{0,1:T(8,128)} %get-tuple-element.35) | copy-start | bytes 196612
  96.3 16.3 %collective-permute-start.1 = (bf16[128,256]{1,0:T(8,128)(2,1)}, bf16[128,256]{1,0:T(8,128)(2,1)}, u32[]{:S(2)}, u32[]{:S(2)}) collective-permute-start(bf16[128,256]{1,0:T(8,128)(2,1)} %get-tuple-element.20), channel_id=1, source_target_pairs={{8,0},{16,8},{24,16},{32,24},{40,32},{48,40},{56,48},{64,56},{72,6... | collective-permute-start | bytes 196616 | tf_op jit(solution)/shard_map/ppermute | solution.py:63
  107.4 4.4 %copy-start.13 = (bf16[512,1,32]{0,2,1:T(8,128)(2,1)S(1)}, bf16[512,1,32]{0,2,1:T(8,128)(2,1)}, u32[]{:S(2)}) copy-start(bf16[512,1,32]{0,2,1:T(8,128)(2,1)} %copy-done.12) | copy-start | bytes 98308
  107.4 4.5 %copy-start.11 = (bf16[512,1,32]{0,2,1:T(8,128)(2,1)S(1)}, bf16[512,1,32]{0,2,1:T(8,128)(2,1)}, u32[]{:S(2)}) copy-start(bf16[512,1,32]{0,2,1:T(8,128)(2,1)} %copy-done.10) | copy-start | bytes 98308
  107.4 4.6 %copy-start.9 = (bf16[512,1,32]{0,2,1:T(8,128)(2,1)S(1)}, bf16[512,1,32]{0,2,1:T(8,128)(2,1)}, u32[]{:S(2)}) copy-start(bf16[512,1,32]{0,2,1:T(8,128)(2,1)} %copy-done.8) | copy-start | bytes 98308
  107.4 4.8 %copy-start.7 = (bf16[512,1,32]{0,2,1:T(8,128)(2,1)S(1)}, bf16[512,1,32]{0,2,1:T(8,128)(2,1)}, u32[]{:S(2)}) copy-start(bf16[512,1,32]{0,2,1:T(8,128)(2,1)} %copy-done.6) | copy-start | bytes 98308
  107.4 6.3 %copy-start.5 = (bf16[4,128,2,128]{3,1,2,0:T(8,128)(2,1)S(1)}, bf16[4,128,2,128]{3,1,2,0:T(8,128)(2,1)}, u32[]{:S(2)}) copy-start(bf16[4,128,2,128]{3,1,2,0:T(8,128)(2,1)} %pad_maximum_fusion.3) | copy-start | bytes 786436
  112.6 2.7 %copy-start.18 = (f32[4,2,128]{2,1,0:T(2,128)S(1)}, f32[4,2,128]{2,1,0:T(2,128)}, u32[]{:S(2)}) copy-start(f32[4,2,128]{2,1,0:T(2,128)} %get-tuple-element.38) | copy-start | bytes 12292
  112.6 2.7 %copy-start.19 = (f32[2]{0:T(128)S(1)}, f32[2]{0:T(128)}, u32[]{:S(2)}) copy-start(f32[2]{0:T(128)} %dynamic_slice.7) | copy-start | bytes 28
  112.6 2.7 %copy-start.1 = (f32[4,1,2,128,1024]{3,4,2,0,1:T(8,128)S(1)}, f32[4,1,2,128,1024]{3,4,2,0,1:T(8,128)}, u32[]{:S(2)}) copy-start(f32[4,1,2,128,1024]{3,4,2,0,1:T(8,128)} %get-tuple-element.39) | copy-start | bytes 12582916
  119.2 44.2 %copy-start.2 = (bf16[64,4096]{1,0:T(8,128)(2,1)S(1)}, bf16[64,4096]{1,0:T(8,128)(2,1)}, u32[]{:S(2)}) copy-start(bf16[64,4096]{1,0:T(8,128)(2,1)} %param.12) | copy-start | bytes 1572868
  (3 other events, 1.8 us)
Sparse Core Ops, SparseCore 0:
  52.6 30.6 all-gather.1
  122.5 40.7 reduce-scatter.1
where the time goes:
time: 173 us; the launch traced here: 172 us
  waiting for transfers between devices  68.7 us (40%)
  matrix products  27.4 us (16%)
  starting transfers between devices  24.4 us (14%)
  other arithmetic  17.3 us (10%)
  between operations  14 us (8%)
  blocking collectives  13.1 us (8%)
  local copies, waits for them, and re-layouts  7.21 us (4%)
    reduce_scatter x1, waiting for transfers between devices, shards(): lax.psum_scatter(jnp.dot(attended, w_out, preferred_element_type=jnp.floa...  40.9 us
    all_gather x1, waiting for transfers between devices, shards(): piece = lax.all_gather(latent_mod, 'tp', axis=0, tiled=True)  17.7 us
    all_to_all x2, starting transfers between devices, sent_to_all(): lax.all_to_all(jnp.broadcast_to(value[None], (length, *value.shape)), axi...  17.6 us
    all_gather x1, blocking collectives, side_by_side(): filled = lax.all_gather(both, axis, axis=dim, tiled=True)  13.1 us
    all_to_all x2, waiting for transfers between devices, sent_to_all(): lax.all_to_all(jnp.broadcast_to(value[None], (length, *value.shape)), axi...  10 us
    dot_general x1, matrix products, shards(): jnp.einsum('nqhgd,khd->nhgqk', query_block_list, context_key_rows, prefer...  4.34 us
    dot_general x1, matrix products, shards(): jnp.dot(piece, w_query, preferred_element_type=jnp.float32)  4.16 us
    dot_general x1, matrix products, shards(): jnp.dot(piece, value_weight, preferred_element_type=jnp.float32)  3.73 us
  transfers between devices with their start and end apart: 6, of which 3 were waited for; matrix products, arithmetic and copies ran while one was open for 18% of the time, Pallas kernels for 0%

commit v1 on v0

--- a/solution.py
+++ b/solution.py
@@ -9,6 +9,12 @@
 EPS = 1e-05
 THETA = 10000.0
 MASKED = -1e30
+
+
+def in_order_2(blocks, dim):
+    shape = list(blocks.shape[1:])
+    shape[dim] *= blocks.shape[0]
+    return jnp.moveaxis(blocks, 0, dim).reshape(shape)
 
 
 def sent_to_all(value, axis):
@@ -152,7 +158,19 @@
         "sp",
         0,
     )
-    piece = lax.all_gather(latent_mod, "tp", axis=0, tiled=True)
+    count_2 = lax.axis_size("tp")
+    pairs = [(i_2, (i_2 + 1) % count_2) for i_2 in range(count_2)]
+    back = [(b, a_2) for a_2, b in pairs]
+    lower, upper = ([], [])
+    for lap in range(count_2 - 1):
+        if lap % 2 == 0:
+            lower.append(lax.ppermute(lower[-1] if lower else latent_mod, "tp", pairs))
+        else:
+            upper.append(lax.ppermute(upper[-1] if upper else latent_mod, "tp", back))
+    parts = jnp.stack([*lower[::-1], latent_mod, *upper])
+    shift_2 = lax.axis_index("tp") - len(lower)
+    parts = parts[(jnp.arange(count_2) - shift_2) % count_2]
+    piece = in_order_2(parts, 0)
     projected_rows = jnp.concatenate(
         [
             jnp.dot(piece, w_query, preferred_element_type=jnp.float32).astype(jnp.bfloat16),

time: 173 us -> 221 us (1.28)
  local copies, waits for them, and re-layouts: 7.21 us -> 46.3 us
  starting transfers between devices: 24.4 us -> 32.7 us
  other arithmetic: 17.3 us -> 20.6 us
    ppermute x0 -> x7, waiting for transfers between devices: none -> 19.7 us  [the longest x4 19.7 us: shards(): lower.append(lax.ppermute(lower[-1] if lower else latent_mod, 'tp', pairs))]
    concatenate x16, local copies, waits for them, and re-layouts: 3.27 us -> 21.8 us  [axial_rotation(): jnp.concatenate([rotate_half(values[..., :width], token_position // grid,...]
    all_gather x1 -> x0, waiting for transfers between devices: 17.7 us -> none  [shards(): piece = lax.all_gather(latent_mod, 'tp', axis=0, tiled=True)]
    unnamed x44, local copies, waits for them, and re-layouts: 0.19 us -> 11.4 us
    ppermute x0 -> x7, starting transfers between devices: none -> 8.66 us  [the longest x3 8.3 us: shards(): upper.append(lax.ppermute(upper[-1] if upper else latent_mod, 'tp', back))]
    gather x0 -> x1, local copies, waits for them, and re-layouts: none -> 4.96 us  [shards(): parts = parts[(jnp.arange(count_2) - shift_2) % count_2]]
    concatenate x2, local copies, waits for them, and re-layouts: 0.48 us -> 3.33 us  [shards(): jnp.concatenate([key.reshape(tokens_here, kv_cols), value_rows], axis=1)]
    dot_general x1, matrix products: 3.73 us -> 1.25 us  [shards(): jnp.dot(piece, value_weight, preferred_element_type=jnp.float32)]
  transfers between devices with their start and end apart: 6 -> 12, of which waited for: 3 -> 5; matrix products, arithmetic and copies ran while one was open for 18% -> 34% of each run, Pallas kernels for 0% -> 0%
where the time goes in v1:
time: 221 us; the launch traced here: 219 us
  waiting for transfers between devices  66.9 us (30%)
  local copies, waits for them, and re-layouts  46.3 us (21%)
  starting transfers between devices  32.7 us (15%)
  matrix products  25.5 us (12%)
  other arithmetic  20.6 us (9%)
  between operations  13.8 us (6%)
  blocking collectives  13.1 us (6%)
    reduce_scatter x1, waiting for transfers between devices, shards(): lax.psum_scatter(jnp.dot(attended, w_out, preferred_element_type=jnp.floa...  39.5 us
    concatenate x16, local copies, waits for them, and re-layouts, axial_rotation(): jnp.concatenate([rotate_half(values[..., :width], token_position // grid,...  21.8 us
    ppermute x4, waiting for transfers between devices, shards(): lower.append(lax.ppermute(lower[-1] if lower else latent_mod, 'tp', pairs))  19.7 us
    all_to_all x2, starting transfers between devices, sent_to_all(): lax.all_to_all(jnp.broadcast_to(value[None], (length, *value.shape)), axi...  17.3 us
    all_gather x1, blocking collectives, side_by_side(): filled = lax.all_gather(both, axis, axis=dim, tiled=True)  13.1 us
    unnamed x44, local copies, waits for them, and re-layouts  11.4 us
    ppermute x3, starting transfers between devices, shards(): upper.append(lax.ppermute(upper[-1] if upper else latent_mod, 'tp', back))  8.3 us
    all_to_all x2, waiting for transfers between devices, sent_to_all(): lax.all_to_all(jnp.broadcast_to(value[None], (length, *value.shape)), axi...  7.61 us
  transfers between devices with their start and end apart: 12, of which 5 were waited for; matrix products, arithmetic and copies ran while one was open for 34% of the time, Pallas kernels for 0%

profile of v1, /device:TPU:8, one launch (start us, length us, event | category | flops | bytes accessed | tf_op | source)
XLA Modules:
  0.0 218.9 jit_solution(7625388339555118393)
XLA Ops:
  11.5 11.7 %all-to-all-start = ((f32[32,1,2560]{2,1,0:T(1,128)}), f32[32,1,2560]{2,1,0:T(1,128)S(1)}, u32[]{:S(2)}, u32[]{:S(2)}) async-start(f32[32,1,2560]{2,1,0:T(1,128)} %broadcast_in_dim.12), calls=%async_computation | async-start | bytes 655360 | tf_op jit(solution)/shard_map/all_to_all | solution.py:22
  28.2 7.6 %all-to-all-done = f32[32,1,2560]{2,1,0:T(1,128)S(1)} async-done(((f32[32,1,2560]{2,1,0:T(1,128)}), f32[32,1,2560]{2,1,0:T(1,128)S(1)}, u32[]{:S(2)}, u32[]{:S(2)}) %all-to-all-start) | async-done | bytes 327712 | tf_op jit(solution)/shard_map/all_to_all | solution.py:22
  36.1 13.1 %all_gather.3 = f32[5,4096]{1,0:T(8,128)S(1)} all-gather(f32[5,512]{1,0:T(8,128)S(1)} %pad_maximum_fusion.4), channel_id=1, replica_groups=mesh['sp'=32,'tp'=8] {'tp'}, dimensions={1}, use_global_device_ids=true | all-gather | bytes 92160 | tf_op jit(solution)/shard_map/all_gather | solution.py:44
  51.2 9.2 %collective-permute-done = bf16[64,4096]{1,0:T(8,128)(2,1)S(1)} collective-permute-done((bf16[64,4096]{1,0:T(8,128)(2,1)S(1)}, bf16[64,4096]{1,0:T(8,128)(2,1)S(1)}, u32[]{:S(2)}, u32[]{:S(2)}) %collective-permute-start) | collective-permute-done | bytes 524320 | tf_op jit(solution)/shard_map/ppermute | solution.py:167
  60.5 3.0 %collective-permute-start.4 = (bf16[64,4096]{1,0:T(8,128)(2,1)S(1)}, bf16[64,4096]{1,0:T(8,128)(2,1)}, u32[]{:S(2)}, u32[]{:S(2)}) collective-permute-start(bf16[64,4096]{1,0:T(8,128)(2,1)S(1)} %fusion.13), channel_id=1, source_target_pairs={{1,0},{2,1},{3,2},{4,3},{5,4},{6,5},{7,6},{0,7},{9,8},{10,9},{11,1... | collective-permute-start | bytes 1572872 | tf_op jit(solution)/shard_map/ppermute | solution.py:169
  63.5 6.7 %collective-permute-done.1 = bf16[64,4096]{1,0:T(8,128)(2,1)S(1)} collective-permute-done((bf16[64,4096]{1,0:T(8,128)(2,1)S(1)}, bf16[64,4096]{1,0:T(8,128)(2,1)S(1)}, u32[]{:S(2)}, u32[]{:S(2)}) %collective-permute-start.1) | collective-permute-done | bytes 524320 | tf_op jit(solution)/shard_map/ppermute | solution.py:167
  70.2 1.9 fusion.16
  73.3 2.9 %collective-permute-start.5 = (bf16[64,4096]{1,0:T(8,128)(2,1)}, bf16[64,4096]{1,0:T(8,128)(2,1)}, u32[]{:S(2)}, u32[]{:S(2)}) collective-permute-start(bf16[64,4096]{1,0:T(8,128)(2,1)} %collective-permute-done.4), channel_id=1, source_target_pairs={{1,0},{2,1},{3,2},{4,3},{5,4},{6,5},{7,6},{0,7},{9,8},{10,9},{11,1... | collective-permute-start | bytes 1572872 | tf_op jit(solution)/shard_map/ppermute | solution.py:169
  76.3 3.8 %collective-permute-done.2 = bf16[64,4096]{1,0:T(8,128)(2,1)} collective-permute-done((bf16[64,4096]{1,0:T(8,128)(2,1)S(1)}, bf16[64,4096]{1,0:T(8,128)(2,1)}, u32[]{:S(2)}, u32[]{:S(2)}) %collective-permute-start.2) | collective-permute-done | bytes 524320 | tf_op jit(solution)/shard_map/ppermute | solution.py:167
  84.2 5.6 %all-to-all-start.1 = ((bf16[32,32,256]{2,1,0:T(8,128)(2,1)}), bf16[32,32,256]{2,1,0:T(8,128)(2,1)S(1)}, u32[]{:S(2)}, u32[]{:S(2)}) async-start(bf16[32,32,256]{2,1,0:T(8,128)(2,1)} %broadcast_in_dim.15), calls=%async_computation.1 | async-start | bytes 1048576 | tf_op jit(solution)/shard_map/all_to_all | solution.py:22
  89.8 2.4 %collective-permute-start.6 = (bf16[64,4096]{1,0:T(8,128)(2,1)}, bf16[64,4096]{1,0:T(8,128)(2,1)S(1)}, u32[]{:S(2)}, u32[]{:S(2)}) collective-permute-start(bf16[64,4096]{1,0:T(8,128)(2,1)} %collective-permute-done.5), channel_id=1, source_target_pairs={{1,0},{2,1},{3,2},{4,3},{5,4},{6,5},{7,6},{0,7},{9,8},{10,9},{11,1... | collective-permute-start | bytes 1572872 | tf_op jit(solution)/shard_map/ppermute | solution.py:169
  96.0 1.9 bitcast_dynamic-update-slice_fusion.5
  97.9 1.9 bitcast_dynamic-update-slice_fusion.4
  105.5 5.0 %gather_fusion = bf16[8,64,4096]{2,1,0:T(8,128)(2,1)} fusion(bf16[8,64,4096]{2,1,0:T(8,128)(2,1)} %bitcast_dynamic-update-slice_fusion, s32[1024]{0:T(1024)S(1)} %pad_clamp_fusion), kind=kCustom, calls=%fused_computation | custom fusion | bytes 8388640 | tf_op jit(solution)/shard_map/gather | solution.py:172
  110.4 4.1 %fusion.9 = f32[512,1,128]{0,2,1:T(8,128)S(1)} fusion(bf16[512,4096]{1,0:T(8,128)(2,1)} %bitcast.141, bf16[4096,128]{1,0:T(8,128)(2,1)} %param.20), kind=kOutput, calls=%fused_computation.23 | convolution fusion | flops 537001984 | bytes 5505024 | tf_op jit(solution)/shard_map/dot_general | solution.py:177
  121.5 3.4 %collective-permute-start.7 = (bf16[128,256]{1,0:T(8,128)(2,1)}, bf16[128,256]{1,0:T(8,128)(2,1)}, u32[]{:S(2)}, u32[]{:S(2)}) collective-permute-start(bf16[128,256]{1,0:T(8,128)(2,1)} %get-tuple-element.19), channel_id=1, source_target_pairs={{0,8},{8,16},{16,24},{24,32},{32,40},{40,48},{48,56},{56,64},{64,7... | collective-permute-start | bytes 196616 | tf_op jit(solution)/shard_map/ppermute | solution.py:67
  124.9 3.4 %collective-permute-start.8 = (bf16[128,256]{1,0:T(8,128)(2,1)}, bf16[128,256]{1,0:T(8,128)(2,1)}, u32[]{:S(2)}, u32[]{:S(2)}) collective-permute-start(bf16[128,256]{1,0:T(8,128)(2,1)} %get-tuple-element.20), channel_id=1, source_target_pairs={{8,0},{16,8},{24,16},{32,24},{40,32},{48,40},{56,48},{64,56},{72,6... | collective-permute-start | bytes 196616 | tf_op jit(solution)/shard_map/ppermute | solution.py:69
  128.3 4.2 %convolution_convert_fusion.1 = bf16[512,256]{0,1:T(8,128)(2,1)S(1)} fusion(bf16[512,4096]{1,0:T(8,128)(2,1)} %bitcast.142, bf16[4096,256]{1,0:T(8,128)(2,1)} %param.19), kind=kOutput, calls=%fused_computation.18 | convolution fusion | flops 1073872896 | bytes 6553600 | tf_op jit(solution)/shard_map/dot_general | solution.py:176
  146.1 2.2 %pad_maximum_fusion.3 = bf16[4,128,2,128]{3,1,2,0:T(8,128)(2,1)} fusion(bf16[4,128,2,32]{3,1,2,0:T(8,128)(2,1)} %copy.71, bf16[4,128,2,32]{3,1,2,0:T(8,128)(2,1)} %copy.70, bf16[4,128,2,32]{3,1,2,0:T(8,128)(2,1)} %copy.69, bf16[4,128,2,32]{3,1,2,0:T(8,128)(2,1)} %copy.68), kind=kLoop, calls=%fused_computation.62 | loop fusion | flops 1048576 | bytes 524288 | tf_op jit(solution)/shard_map/concatenate | solution.py:99
  148.3 4.2 %fusion.61 = (f32[4,2,128]{2,1,0:T(2,128)}, f32[4,1,2,128,1024]{3,4,2,0,1:T(8,128)}) fusion(bf16[4,128,2,128]{3,1,2,0:T(8,128)(2,1)} %pad_maximum_fusion.3, bf16[1024,256]{1,0:T(8,128)(2,1)S(1)} %bitcast.144), kind=kOutput, calls=%fused_computation.139 | convolution fusion | flops 270531584 | bytes 4722688 | tf_op jit(solution)/shard_map/nqhgd,khd->nhgqk/dot_general | solution.py:237
  158.6 2.0 concatenate.95
  167.3 3.2 %convolution_convert_fusion = bf16[512,4096]{1,0:T(8,128)(2,1)} fusion(bf16[256,4096]{1,0:T(8,128)(2,1)S(1)} %copy-done, bf16[64,8,2,128]{3,2,1,0:T(2,128)(2,1)S(1)} %bitcast.146), kind=kOutput, calls=%fused_computation.1 | convolution fusion | flops 1075838976 | bytes 6553600 | tf_op jit(solution)/shard_map/dot_general | solution.py:262
  170.5 39.5 %reduce-scatter.2.cloned.1.call-done = bf16[64,4096]{1,0:T(8,128)(2,1)} async-done(((bf16[512,4096]{1,0:T(8,128)(2,1)}), bf16[64,4096]{1,0:T(8,128)(2,1)}) %reduce-scatter.2.cloned.1.call-update) | async-done | bytes 524304 | tf_op jit(solution)/shard_map/reduce_scatter | solution.py:261
  210.1 2.0 fusion.14
  (125 shorter events, 60.2 us)
Async XLA Ops:
  6.5 160.8 %copy-start = (bf16[256,4096]{1,0:T(8,128)(2,1)S(1)}, bf16[256,4096]{1,0:T(8,128)(2,1)}, u32[]{:S(2)}) copy-start(bf16[256,4096]{1,0:T(8,128)(2,1)} %param.22) | copy-start | bytes 6291460
  6.5 44.4 %copy-start.4 = (bf16[32,4096]{1,0:T(8,128)(2,1)S(1)}, bf16[32,4096]{1,0:T(8,128)(2,1)}, u32[]{:S(2)}) copy-start(bf16[32,4096]{1,0:T(8,128)(2,1)} %param.13) | copy-start | bytes 786436
  11.5 24.3 %all-to-all-start = ((f32[32,1,2560]{2,1,0:T(1,128)}), f32[32,1,2560]{2,1,0:T(1,128)S(1)}, u32[]{:S(2)}, u32[]{:S(2)}) async-start(f32[32,1,2560]{2,1,0:T(1,128)} %broadcast_in_dim.12), calls=%async_computation | async-start | bytes 655360 | tf_op jit(solution)/shard_map/all_to_all | solution.py:22
  50.5 9.8 %collective-permute-start = (bf16[64,4096]{1,0:T(8,128)(2,1)S(1)}, bf16[64,4096]{1,0:T(8,128)(2,1)S(1)}, u32[]{:S(2)}, u32[]{:S(2)}) collective-permute-start(bf16[64,4096]{1,0:T(8,128)(2,1)S(1)} %fusion.13), channel_id=1, source_target_pairs={{0,1},{1,2},{2,3},{3,4},{4,5},{5,6},{6,7},{7,0},{8,9},{9,10},{10,1... | collective-permute-start | bytes 1572872 | tf_op jit(solution)/shard_map/ppermute | solution.py:167
  60.4 22.9 %copy-start.6 = (bf16[64,4096]{1,0:T(8,128)(2,1)}, bf16[64,4096]{1,0:T(8,128)(2,1)S(1)}, u32[]{:S(2)}) copy-start(bf16[64,4096]{1,0:T(8,128)(2,1)S(1)} %collective-permute-done) | copy-start | bytes 1572868
  60.4 9.8 %collective-permute-start.1 = (bf16[64,4096]{1,0:T(8,128)(2,1)S(1)}, bf16[64,4096]{1,0:T(8,128)(2,1)S(1)}, u32[]{:S(2)}, u32[]{:S(2)}) collective-permute-start(bf16[64,4096]{1,0:T(8,128)(2,1)S(1)} %collective-permute-done), channel_id=1, source_target_pairs={{0,1},{1,2},{2,3},{3,4},{4,5},{5,6},{6,7},{7,0},{8,9},{9,10},{10,1... | collective-permute-start | bytes 1572872 | tf_op jit(solution)/shard_map/ppermute | solution.py:167
  60.5 12.8 %collective-permute-start.4 = (bf16[64,4096]{1,0:T(8,128)(2,1)S(1)}, bf16[64,4096]{1,0:T(8,128)(2,1)}, u32[]{:S(2)}, u32[]{:S(2)}) collective-permute-start(bf16[64,4096]{1,0:T(8,128)(2,1)S(1)} %fusion.13), channel_id=1, source_target_pairs={{1,0},{2,1},{3,2},{4,3},{5,4},{6,5},{7,6},{0,7},{9,8},{10,9},{11,1... | collective-permute-start | bytes 1572872 | tf_op jit(solution)/shard_map/ppermute | solution.py:169
  70.2 13.1 %copy-start.7 = (bf16[64,4096]{1,0:T(8,128)(2,1)}, bf16[64,4096]{1,0:T(8,128)(2,1)S(1)}, u32[]{:S(2)}) copy-start(bf16[64,4096]{1,0:T(8,128)(2,1)S(1)} %collective-permute-done.1) | copy-start | bytes 1572868
  70.2 9.9 %collective-permute-start.2 = (bf16[64,4096]{1,0:T(8,128)(2,1)S(1)}, bf16[64,4096]{1,0:T(8,128)(2,1)}, u32[]{:S(2)}, u32[]{:S(2)}) collective-permute-start(bf16[64,4096]{1,0:T(8,128)(2,1)S(1)} %collective-permute-done.1), channel_id=1, source_target_pairs={{0,1},{1,2},{2,3},{3,4},{4,5},{5,6},{6,7},{7,0},{8,9},{9,10},{10,1... | collective-permute-start | bytes 1572872 | tf_op jit(solution)/shard_map/ppermute | solution.py:167
  73.3 16.5 %collective-permute-start.5 = (bf16[64,4096]{1,0:T(8,128)(2,1)}, bf16[64,4096]{1,0:T(8,128)(2,1)}, u32[]{:S(2)}, u32[]{:S(2)}) collective-permute-start(bf16[64,4096]{1,0:T(8,128)(2,1)} %collective-permute-done.4), channel_id=1, source_target_pairs={{1,0},{2,1},{3,2},{4,3},{5,4},{6,5},{7,6},{0,7},{9,8},{10,9},{11,1... | collective-permute-start | bytes 1572872 | tf_op jit(solution)/shard_map/ppermute | solution.py:169
  80.1 12.1 %collective-permute-start.3 = (bf16[64,4096]{1,0:T(8,128)(2,1)}, bf16[64,4096]{1,0:T(8,128)(2,1)}, u32[]{:S(2)}, u32[]{:S(2)}) collective-permute-start(bf16[64,4096]{1,0:T(8,128)(2,1)} %collective-permute-done.2), channel_id=1, source_target_pairs={{0,1},{1,2},{2,3},{3,4},{4,5},{5,6},{6,7},{7,0},{8,9},{9,10},{10,1... | collective-permute-start | bytes 1572872 | tf_op jit(solution)/shard_map/ppermute | solution.py:167
  80.1 19.7 %copy-start.3 = (bf16[64,4096]{1,0:T(8,128)(2,1)S(1)}, bf16[64,4096]{1,0:T(8,128)(2,1)}, u32[]{:S(2)}) copy-start(bf16[64,4096]{1,0:T(8,128)(2,1)} %param.12) | copy-start | bytes 1572868
  84.2 64.1 %all-to-all-start.1 = ((bf16[32,32,256]{2,1,0:T(8,128)(2,1)}), bf16[32,32,256]{2,1,0:T(8,128)(2,1)S(1)}, u32[]{:S(2)}, u32[]{:S(2)}) async-start(bf16[32,32,256]{2,1,0:T(8,128)(2,1)} %broadcast_in_dim.15), calls=%async_computation.1 | async-start | bytes 1048576 | tf_op jit(solution)/shard_map/all_to_all | solution.py:22
  89.8 120.3 %reduce-scatter.2.cloned.1.call-start = ((), (), s32[]{:S(2)}) async-start(), calls=%async_computation.3 | async-start | bytes 4718592 | tf_op jit(solution)/shard_map/reduce_scatter | solution.py:261
  89.8 14.8 %collective-permute-start.6 = (bf16[64,4096]{1,0:T(8,128)(2,1)}, bf16[64,4096]{1,0:T(8,128)(2,1)S(1)}, u32[]{:S(2)}, u32[]{:S(2)}) collective-permute-start(bf16[64,4096]{1,0:T(8,128)(2,1)} %collective-permute-done.5), channel_id=1, source_target_pairs={{1,0},{2,1},{3,2},{4,3},{5,4},{6,5},{7,6},{0,7},{9,8},{10,9},{11,1... | collective-permute-start | bytes 1572872 | tf_op jit(solution)/shard_map/ppermute | solution.py:169
  110.4 4.2 %copy-start.2 = (bf16[8,64,4096]{2,1,0:T(8,128)(2,1)S(1)}, bf16[8,64,4096]{2,1,0:T(8,128)(2,1)}, u32[]{:S(2)}) copy-start(bf16[8,64,4096]{2,1,0:T(8,128)(2,1)} %gather_fusion) | copy-start | bytes 12582916
  110.4 4.2 %copy-start.5 = (bf16[4096,128]{1,0:T(8,128)(2,1)S(1)}, bf16[4096,128]{1,0:T(8,128)(2,1)}, u32[]{:S(2)}) copy-start(bf16[4096,128]{1,0:T(8,128)(2,1)} %param.21) | copy-start | bytes 3145732
  121.5 39.1 %collective-permute-start.7 = (bf16[128,256]{1,0:T(8,128)(2,1)}, bf16[128,256]{1,0:T(8,128)(2,1)}, u32[]{:S(2)}, u32[]{:S(2)}) collective-permute-start(bf16[128,256]{1,0:T(8,128)(2,1)} %get-tuple-element.19), channel_id=1, source_target_pairs={{0,8},{8,16},{16,24},{24,32},{32,40},{40,48},{48,56},{56,64},{64,7... | collective-permute-start | bytes 196616 | tf_op jit(solution)/shard_map/ppermute | solution.py:67
  124.9 7.6 %copy-start.12 = (f32[512,32]{0,1:T(8,128)S(1)}, f32[512,32]{0,1:T(8,128)}, u32[]{:S(2)}) copy-start(f32[512,32]{0,1:T(8,128)} %get-tuple-element.28) | copy-start | bytes 196612
  124.9 7.6 %copy-start.13 = (f32[512,32]{0,1:T(8,128)S(1)}, f32[512,32]{0,1:T(8,128)}, u32[]{:S(2)}) copy-start(f32[512,32]{0,1:T(8,128)} %get-tuple-element.29) | copy-start | bytes 196612
  124.9 7.6 %copy-start.14 = (f32[512,32]{0,1:T(8,128)S(1)}, f32[512,32]{0,1:T(8,128)}, u32[]{:S(2)}) copy-start(f32[512,32]{0,1:T(8,128)} %get-tuple-element.34) | copy-start | bytes 196612
  124.9 7.6 %copy-start.15 = (f32[512,32]{0,1:T(8,128)S(1)}, f32[512,32]{0,1:T(8,128)}, u32[]{:S(2)}) copy-start(f32[512,32]{0,1:T(8,128)} %get-tuple-element.35) | copy-start | bytes 196612
  124.9 35.7 %collective-permute-start.8 = (bf16[128,256]{1,0:T(8,128)(2,1)}, bf16[128,256]{1,0:T(8,128)(2,1)}, u32[]{:S(2)}, u32[]{:S(2)}) collective-permute-start(bf16[128,256]{1,0:T(8,128)(2,1)} %get-tuple-element.20), channel_id=1, source_target_pairs={{8,0},{16,8},{24,16},{32,24},{40,32},{48,40},{56,48},{64,56},{72,6... | collective-permute-start | bytes 196616 | tf_op jit(solution)/shard_map/ppermute | solution.py:69
  160.6 3.8 %copy-start.1 = (f32[4,1,2,128,1024]{3,4,2,0,1:T(8,128)S(1)}, f32[4,1,2,128,1024]{3,4,2,0,1:T(8,128)}, u32[]{:S(2)}) copy-start(f32[4,1,2,128,1024]{3,4,2,0,1:T(8,128)} %get-tuple-element.39) | copy-start | bytes 12582916
  (6 other events, 16.8 us)
Sparse Core Ops, SparseCore 0:
  170.7 39.3 reduce-scatter.1
